TPU v7x, 512 devices: a whole 4x4x16 slice. The times are simulated.
512 devices in a mesh: ep: 16 (over y, x), tp: 32 (over z, core).
Axes of the slice: x: 4, y: 4, z: 16, core: 2. Of those that a mesh axis runs over, the one named last changes fastest.
Arguments:
- tokens: bfloat16 [3072, 2048], P('ep'), may hold values from -6 to 6
- cotangent: bfloat16 [3072, 2048], P('ep'), may hold values from -6 to 6
- routes: int32 [3072, 2], P('ep'), may hold values from 0 to 15, all different within a row; in each aligned block of 192 rows (0 to 191, 192 to 383, ...) at most 48 rows name the same one
- route_weight: float32 [3072, 2], P('ep'), may hold values from 0.2 to 1
- gate_weight: bfloat16 [16, 2048, 4096], P('ep', None, 'tp'), may hold values from -0.125 to 0.125
- up_weight: bfloat16 [16, 2048, 4096], P('ep', None, 'tp'), may hold values from -0.125 to 0.125
- down_weight: bfloat16 [16, 4096, 2048], P('ep', 'tp'), may hold values from -0.09375 to 0.09375
Outputs:
- grad_tokens: bfloat16 [3072, 2048], P('ep', 'tp')
- grad_route: float32 [3072, 2], P('ep')
- grad_gate: bfloat16 [16, 2048, 4096], P('ep', None, 'tp')
- grad_up: bfloat16 [16, 2048, 4096], P('ep', None, 'tp')
- grad_down: bfloat16 [16, 4096, 2048], P('ep', 'tp')
Inputs may be any that keep to these rules, and one draw needn't show every extreme that they name: `routes`: within the rows of one device along ep, each expert is named at most 48 times, a bound that some block reaches; the 2 entries of a row differ.
All inputs are finite; a program needn't handle non-finite values.
Results may differ from a plain program's by a relative error of at most 0.025.
Values may be sent and summed in bfloat16 or wider, within the bound.
No kernel may reach another device: no remote copies, remote signals or barrier semaphores. Data moves between devices by JAX's collectives and lax.ppermute only.
A program may use at most 64 MiB of HBM per device.

v0:
```python
import functools

import jax
import jax.numpy as jnp
from jax import lax
from jax.experimental import pallas as pl
from jax.experimental.pallas import tpu as pltpu
from jax.sharding import Mesh
from jax.sharding import PartitionSpec as P


BF = jnp.bfloat16
F32 = jnp.float32
TP = ("zh", "zl", "core")
LANES = 128
OWN = 64


def dot(a, b, ca=1, cb=0):
    return lax.dot_general(a, b, (((ca,), (cb,)), ((), ())), preferred_element_type=F32)


def split(v):
    hi = v.astype(BF)
    return hi, (v - hi.astype(F32)).astype(BF)


def padded(v, width):
    return jnp.concatenate([v, jnp.zeros((v.shape[0], width - v.shape[1]), v.dtype)], axis=1)


def stacked(rows, height):
    place = lax.broadcasted_iota(jnp.int32, (height, rows[0].shape[1]), 0)
    out = jnp.zeros(place.shape, F32)
    for k, row in enumerate(rows):
        out = jnp.where(place == k, row.astype(F32), out)
    return out


def ranks(routes, experts):
    rows = routes.shape[1]
    ids = lax.broadcasted_iota(jnp.int32, (experts, rows), 0)
    first, second = routes[0:1] == ids, routes[1:2] == ids
    named = first | second
    before = lax.broadcasted_iota(jnp.int32, (rows, rows), 0) < lax.broadcasted_iota(
        jnp.int32, (rows, rows), 1
    )
    one, zero = jnp.ones((), F32), jnp.zeros((), F32)
    count = dot(jnp.where(named, one, zero).astype(BF), jnp.where(before, one, zero).astype(BF))
    return first, second, jnp.where(named, count, -one)


def vmem(n):
    return [pl.BlockSpec(memory_space=pltpu.VMEM)] * n


def call(kernel, out, scratch, limit, flops, *args, space=pltpu.VMEM):
    return pl.pallas_call(
        kernel,
        in_specs=[pl.BlockSpec(memory_space=pltpu.SMEM)]
        + [pl.BlockSpec(memory_space=space)] * (len(args) - 1),
        out_specs=vmem(len(out)),
        out_shape=out,
        scratch_shapes=scratch,
        compiler_params=pltpu.CompilerParams(vmem_limit_bytes=limit << 20),
        cost_estimate=pl.CostEstimate(flops=flops, bytes_accessed=flops // 400, transcendentals=0),
    )(args[0], *[pltpu.with_memory_space_constraint(a, space) if space == pltpu.HBM else a for a in args[1:]])


def struct(*shape, dtype=BF):
    return jax.ShapeDtypeStruct(shape, dtype)


def loads(pairs, sems):
    copies = [pltpu.make_async_copy(src, dst, sems.at[k]) for k, (src, dst) in enumerate(pairs)]
    for copy in copies:
        copy.start()
    return copies


def gather_lanes(x, core, nzl, out, col):
    n = x.shape[1] // LANES // nzl // 2
    for own in range(2):

        @pl.when(core == own)
        def _():
            for zl in range(nzl):
                for q in range(n):
                    at = [((2 * q + k) * nzl + zl) * LANES + own * OWN for k in range(2)]
                    pair = [x[:, pl.ds(p, OWN)] for p in at]
                    out[:, pl.ds(col + (zl * n + q) * LANES, LANES)] = jnp.concatenate(pair, axis=1)


def blocks(core, nzh, nzl):
    for zl in range(nzl):
        for zh in range(nzh):
            yield pl.ds((zl * nzh + zh) * OWN, OWN), pl.ds(
                pl.multiple_of(((zh * nzl + zl) * 2 + core) * OWN, OWN), OWN
            )


def prepare_kernel(core, routes_h, weights_h, gate_h, up_h, down_h, x_h, c_h,
                   routes, weights, x, c, w_own, w_oth,
                   gate, up, down, turned, sems, *, nzh, nzl):
    copies = loads(
        (
            (gate_h, gate),
            (up_h, up),
            (down_h, down),
            (routes_h, routes),
            (weights_h, weights),
            (x_h, x),
            (c_h, c),
        ),
        sems,
    )
    for k, src in enumerate((gate, up, turned)):
        copies[k].wait()
        if k == 2:
            turned[...] = down[...].T
        for to_ref, who in ((w_oth, 1 - core[0]), (w_own, core[0])):
            for to, at in blocks(who, nzh, nzl):
                to_ref[to, pl.ds(k * LANES, LANES)] = src[at, :]
    for copy in copies[3:]:
        copy.wait()


def prepare(core, routes, weights, gate, up, down, tokens, cot, nzh, nzl):
    rows, d = tokens.shape
    return call(
        functools.partial(prepare_kernel, nzh=nzh, nzl=nzl),
        [struct(*routes.shape, dtype=jnp.int32), struct(*weights.shape, dtype=F32)]
        + [struct(rows, d)] * 2
        + [struct(d // 2, 3 * LANES)] * 2,
        [
            pltpu.VMEM((d, LANES), BF),
            pltpu.VMEM((d, LANES), BF),
            pltpu.VMEM((LANES, d), BF),
            pltpu.VMEM((d, LANES), BF),
            pltpu.SemaphoreType.DMA((7,)),
        ],
        16, 1 << 28, core, routes, weights, gate, up, down, tokens, cot, space=pltpu.HBM,
    )


def pack_kernel(core, routes, weights, x, c, out, sel, xo, wsel, *, experts, cap, nzl):
    half = x.shape[1] // 2
    first, second, rank = ranks(routes[...], experts)
    w = weights[...]
    mine = jnp.where(first, w[0:1], 0.0) + jnp.where(second, w[1:2], 0.0)
    slot = lax.broadcasted_iota(jnp.int32, (cap, rank.shape[1]), 0).astype(F32)
    for e in range(experts):
        hit = rank[e : e + 1] == slot
        sel[pl.ds(e * cap, cap), :] = jnp.where(hit, 1.0, 0.0).astype(BF)
        wsel[pl.ds(e * cap, cap), :] = jnp.where(hit, mine[e : e + 1], 0.0).astype(BF)
    gather_lanes(x, core[0], nzl, xo, 0)
    gather_lanes(c, core[0], nzl, xo, half)
    out[:, pl.ds(0, half)] = dot(sel[...], xo[:, pl.ds(0, half)]).astype(BF)
    out[:, pl.ds(half, half)] = dot(wsel[...], xo[:, pl.ds(half, half)]).astype(BF)


def pack(core, routes, weights, x, c, experts, cap, nzl):
    rows, d = x.shape
    slots = experts * cap
    return call(
        functools.partial(pack_kernel, experts=experts, cap=cap, nzl=nzl),
        [struct(slots, d), struct(slots, rows)],
        [pltpu.VMEM((rows, d), BF), pltpu.VMEM((slots, rows), BF)],
        12, 2 * slots * rows * d, core, routes, weights, x, c,
    )


def forward_kernel(core, own, w_own, w_got, out):
    half = own.shape[1] // 2
    for k, w in enumerate((w_own, w_got)):
        col = 3 * LANES * k
        out[:, pl.ds(col, 2 * LANES)] = dot(own[:, pl.ds(0, half)], w[:, pl.ds(0, 2 * LANES)]).astype(BF)
    down = jnp.concatenate([w[:, pl.ds(2 * LANES, LANES)] for w in (w_own, w_got)], axis=1)
    back = dot(own[:, pl.ds(half, half)], down).astype(BF)
    out[:, pl.ds(2 * LANES, LANES)] = back[:, :LANES]
    out[:, pl.ds(5 * LANES, LANES)] = back[:, LANES:]


def forward(core, own, w_own, w_got):
    slots, d = own.shape
    return call(
        forward_kernel, [struct(slots, 6 * LANES)], [], 20, 6 * slots * d * LANES,
        core, own, w_own, w_got,
    )[0]


def backward_kernel(core, part, got, w_own, w_got, hid, dd, out, *, cap, nzl):
    slots = part.shape[0]
    half = w_own.shape[0]
    per = half // nzl // LANES
    lane = 3 * LANES
    group = slots // 2 if slots % (2 * cap) == 0 else slots
    for i in range(slots // group):
        at = pl.ds(i * group, group)
        route = None
        for k in range(2):

            def total(j):
                cols = [pl.ds(lane * side + LANES * j, LANES) for side in (k, 1 - k)]
                return part[at, cols[0]].astype(F32) + got[at, cols[1]].astype(F32)

            a, b, back = total(0), total(1), total(2)
            s = jax.nn.sigmoid(a)
            act = a * s
            hidden = (act * b).astype(BF)
            hid[at, pl.ds(k * LANES, LANES)] = hidden
            dd[at, pl.ds(2 * k * LANES, LANES)] = (back * b * s * (1.0 + a * (1.0 - s))).astype(BF)
            dd[at, pl.ds((2 * k + 1) * LANES, LANES)] = (back * act).astype(BF)
            one = jnp.sum((hidden.astype(F32) * back).T, axis=0, keepdims=True)
            route = one if route is None else route + one
        rows = dot(dd[at, pl.ds(0, 2 * LANES)], w_own[:, pl.ds(0, 2 * LANES)], 1, 1)
        rows = rows + dot(dd[at, pl.ds(2 * LANES, 2 * LANES)], w_got[:, pl.ds(0, 2 * LANES)], 1, 1)
        rows = rows.astype(BF)
        for j in range(group // cap):
            b = i * (group // cap) + j
            ends = stacked(split(padded(route[:, j * cap : (j + 1) * cap], LANES)), 8).astype(BF)
            for zl in range(nzl):
                for q in range(per):
                    k = zl * per + q
                    out[b * nzl + zl, pl.ds(q * cap, cap), :] = rows[
                        j * cap : (j + 1) * cap, k * LANES : (k + 1) * LANES
                    ]
                out[b * nzl + zl, pl.ds(per * cap, 8), :] = ends


def backward(core, part, got, w_own, w_got, nzl, cap):
    slots, half = part.shape[0], w_own.shape[0]
    tall = half // nzl // LANES * cap + 8
    return call(
        functools.partial(backward_kernel, cap=cap, nzl=nzl),
        [
            struct(slots, 2 * LANES),
            struct(slots, 4 * LANES),
            struct(slots // cap * nzl, tall, LANES),
        ],
        [], 24, 8 * slots * half * LANES, core, part, got, w_own, w_got,
    )


def grads_kernel(core, own, hid, dd, keep, send):
    half = own.shape[1] // 2
    both = dot(own[:, pl.ds(0, half)], dd[...], 0, 0)
    keep[:, pl.ds(0, 2 * LANES)] = both[:, : 2 * LANES].astype(BF)
    send[:, pl.ds(0, 2 * LANES)] = both[:, 2 * LANES :].astype(BF)
    down = dot(own[:, pl.ds(half, half)], hid[...], 0, 0)
    keep[:, pl.ds(2 * LANES, LANES)] = down[:, :LANES].astype(BF)
    send[:, pl.ds(2 * LANES, LANES)] = down[:, LANES:].astype(BF)


def grads(core, own, hid, dd):
    slots, d = own.shape
    return call(
        grads_kernel, [struct(d // 2, 3 * LANES)] * 2, [], 24,
        6 * slots * d * LANES, core, own, hid, dd,
    )


def place_kernel(core, keep, got, gg, gu, gd, turned, *, nzh, nzl):
    for k, out in enumerate((gg, gu, turned)):
        for src, who in ((keep, core[0]), (got, 1 - core[0])):
            for at, to in blocks(who, nzh, nzl):
                out[to, :] = src[at, pl.ds(k * LANES, LANES)]
    gd[...] = turned[...].T


def place(core, keep, got, nzh, nzl):
    d = 2 * keep.shape[0]
    return call(
        functools.partial(place_kernel, nzh=nzh, nzl=nzl),
        [struct(d, LANES), struct(d, LANES), struct(LANES, d)],
        [pltpu.VMEM((d, LANES), BF)],
        12, 1 << 28, core, keep, got,
    )


def combine_kernel(routes, weights, sel, got, out, part, *, experts, cap, nzl):
    rows = routes.shape[1]
    per = (got.shape[1] - 8) // cap
    s = sel[...]
    total = None
    for zl in range(nzl):
        for e in range(experts):
            for q in range(per):
                part[zl, pl.ds(e * cap, cap), pl.ds(q * LANES, LANES)] = got[
                    e * nzl + zl, pl.ds(q * cap, cap), :
                ]
        one = dot(s, part[zl], 0, 0)
        total = one if total is None else total + one
    total = total.astype(BF)
    mid = rows // 2
    for k in range(out.shape[0]):
        out[k, pl.ds(0, mid), :] = jnp.concatenate(
            [total[:mid, k * OWN : (k + 1) * OWN], total[mid:, k * OWN : (k + 1) * OWN]], axis=1
        )
    lines = []
    for e in range(experts):
        line = jnp.zeros((1, LANES), F32)
        for zl in range(nzl):
            tail = got[e * nzl + zl, pl.ds(per * cap, 8), :].astype(F32)
            line = line + tail[0:1] + tail[1:2]
        lines.append(line)
    r_hi, r_lo = split(stacked(lines, max(experts, 8)))
    first, second, rank = ranks(routes[...], experts)
    slot = lax.broadcasted_iota(jnp.int32, (LANES, rows), 0).astype(F32)
    ends = []
    wide = -(-rows // LANES) * LANES
    for ch, hit in enumerate((first, second)):
        place = jnp.sum(jnp.where(hit, rank, 0.0), axis=0, keepdims=True)
        pick = jnp.where(slot == place, 1.0, 0.0).astype(BF)
        value = (dot(r_hi, pick) + dot(r_lo, pick))[:experts]
        value = jnp.sum(jnp.where(hit, value, 0.0), axis=0, keepdims=True)
        w = weights[...][ch : ch + 1].astype(BF).astype(F32)
        for piece in split(padded(value / w, wide) if wide > rows else value / w):
            for k in range(wide // LANES):
                ends.append(piece[:, k * LANES : (k + 1) * LANES])
    ends = stacked(ends, 8).astype(BF)
    for k in range(out.shape[0]):
        out[k, pl.ds(mid, 8), :] = ends


def combine(routes, weights, sel, got, experts, cap, nzh, nzl):
    rows = routes.shape[1]
    per = (got.shape[1] - 8) // cap
    return pl.pallas_call(
        functools.partial(combine_kernel, experts=experts, cap=cap, nzl=nzl),
        out_shape=jax.ShapeDtypeStruct((nzh, rows // 2 + 8, LANES), BF),
        in_specs=vmem(4),
        out_specs=vmem(1)[0],
        scratch_shapes=[pltpu.VMEM((nzl, experts * cap, per * LANES), BF)],
        compiler_params=pltpu.CompilerParams(vmem_limit_bytes=16 << 20),
        name="combine",
    )(routes, weights, sel, got)


def finish_kernel(got, grad, route):
    rows = grad.shape[1]
    total = got[0].astype(F32)
    for k in range(1, got.shape[0]):
        total = total + got[k].astype(F32)
    mid = rows // 2
    turned = total[:mid].T
    grad[...] = jnp.concatenate([turned[:OWN], turned[OWN:]], axis=1).astype(BF)
    ends = total[mid:]
    n = -(-rows // LANES)
    for ch in range(2):
        pieces = [
            ends[2 * n * ch + k : 2 * n * ch + k + 1] + ends[2 * n * ch + n + k : 2 * n * ch + n + k + 1]
            for k in range(n)
        ]
        line = jnp.concatenate(pieces, axis=1) if n > 1 else pieces[0]
        route[pl.ds(ch, 1), :] = line[:, :rows]


def finish(got, rows):
    return pl.pallas_call(
        finish_kernel,
        out_shape=[
            jax.ShapeDtypeStruct((OWN, rows), BF),
            jax.ShapeDtypeStruct((2, rows), F32),
        ],
        in_specs=vmem(1),
        out_specs=vmem(2),
        compiler_params=pltpu.CompilerParams(vmem_limit_bytes=8 << 20),
        name="finish",
    )(got)


def shards(tokens, cotangent, routes, route_weight, gate_weight, up_weight, down_weight):
    rows, d = tokens.shape
    experts = lax.axis_size("ep")
    nzh, nzl = lax.axis_size("zh"), lax.axis_size("zl")
    cap = 2 * rows * routes.shape[1] // experts
    slots = experts * cap
    core = lax.axis_index("core").astype(jnp.int32).reshape(1)
    routes_t, weight_t = routes.T, route_weight.T
    gate, up, down = gate_weight[0], up_weight[0], down_weight[0]
    swap = [(0, 1), (1, 0)]

    routes_v, weight_v, x_v, c_v, w_own, w_oth = prepare(
        core, routes_t, weight_t, gate, up, down, tokens, cotangent, nzh, nzl
    )
    w_got = lax.ppermute(w_oth, "core", swap)
    packed, sel = pack(core, routes_v, weight_v, x_v, c_v, experts, cap, nzl)
    packed, w_own, w_got = lax.optimization_barrier((packed, w_own, w_got))
    own = lax.all_to_all(packed.reshape(experts, cap, d), "ep", 0, 0, tiled=True).reshape(slots, d)
    part = forward(core, own, w_own, w_got)
    got = lax.ppermute(part, "core", swap)
    hid, dd, message = backward(core, part, got, w_own, w_got, nzl, cap)
    keep, send = grads(core, own, hid, dd)
    moved = lax.ppermute(send, "core", swap)
    gg, gu, gd = place(core, keep, moved, nzh, nzl)
    back = lax.all_to_all(message, ("ep", "zl"), 0, 0, tiled=True)
    partial = combine(routes_v, weight_v, sel, back, experts, cap, nzh, nzl)
    last = lax.all_to_all(partial, "zh", 0, 0, tiled=True)
    grad_t, route_t = finish(last, rows)
    return grad_t.T, route_t.T, gg[None], gu[None], gd[None]


def solution(mesh):
    devices = mesh.devices
    ep = devices.shape[0]
    finer = Mesh(devices.reshape(ep, -1, 2, 2), ("ep", "zh", "zl", "core"))
    in_specs = (
        P("ep", None),
        P("ep", None),
        P("ep", None),
        P("ep", None),
        P("ep", None, TP),
        P("ep", None, TP),
        P("ep", TP, None),
    )
    out_specs = (
        P("ep", TP),
        P("ep", None),
        P("ep", None, TP),
        P("ep", None, TP),
        P("ep", TP, None),
    )
    return jax.shard_map(
        shards, mesh=finer, in_specs=in_specs, out_specs=out_specs, check_vma=False
    )
```

profile of v0, /device:TPU:32, one launch (start us, length us, event | category | flops | bytes accessed | tf_op | source)
XLA Modules:
  0.0 128.5 jit_solution(16258399136024774421)
XLA Ops:
  0.6 1.9 %shard_map.110 = (s32[2,192]{1,0:T(2,128)S(1)}, f32[2,192]{1,0:T(2,128)S(1)}, bf16[192,2048]{1,0:T(8,128)(2,1)S(1)}, bf16[192,2048]{1,0:T(8,128)(2,1)S(1)}, bf16...) custom-call(s32[1]{0:T(128)} %bitcast.core, s32[2,192]{1,0:T(2,128)} %bitcast.19, f32[2,192]{1,0:T(2,128)} %bitcast.20, ...), custom_call_target="tpu_custom_call" | custom-call | flops 268435456 | bytes 671088 | tf_op jit(solution)/shard_map/pallas_call | solution.py:58
  2.6 1.9 %collective-permute-start = (bf16[1024,384]{1,0:T(8,128)(2,1)S(1)}, bf16[1024,384]{1,0:T(8,128)(2,1)S(1)}, u32[]{:S(2)}, u32[]{:S(2)}) collective-permute-start(bf16[1024,384]{1,0:T(8,128)(2,1)S(1)} %get-tuple-element.33), channel_id=1, source_target_pairs={{0,1},{1,0},{2,3},{3,2},{4,5},{5,4},{6,7},{7,6},{8,9},{9,8},{10,11... | collective-permute-start | bytes 2359304 | tf_op jit(solution)/shard_map/ppermute | solution.py:387
  4.5 1.6 %shard_map.111 = (bf16[768,2048]{1,0:T(8,128)(2,1)S(1)}, bf16[768,192]{1,0:T(8,128)(2,1)S(1)}) custom-call(s32[1]{0:T(128)} %bitcast.core, s32[2,192]{1,0:T(2,128)S(1)} %get-tuple-element.26.routes, f32[2,192]{1,0:T(2,128)S(1)} %get-tuple-element.27.weights, bf16[192,2048]{1,0:T(8,128)(2,1)S(1)} %get-tuple-element.28.x, ...), custom_call_target="tpu_custom_call" | custom-call | flops 603979776 | bytes 1509949 | tf_op jit(solution)/shard_map/pallas_call | solution.py:58
  6.1 0.6 collective-permute-done.w_got
  6.8 46.7 %all_to_all.15 = bf16[16,48,2048]{2,1,0:T(8,128)(2,1)S(1)} all-to-all(bf16[16,48,2048]{2,1,0:T(8,128)(2,1)S(1)} %bitcast.15), channel_id=1, replica_groups=mesh['ep'=16,'zh'=8,'zl'=2,'core'=2] {'ep'}, dimensions={0} | all-to-all | bytes 6291456 | tf_op jit(solution)/shard_map/all_to_all | solution.py:390
  53.5 1.4 %shard_map.112.part = bf16[768,768]{1,0:T(8,128)(2,1)S(1)} custom-call(s32[1]{0:T(128)} %bitcast.core, bf16[768,2048]{1,0:T(8,128)(2,1)S(1)} %bitcast.13, bf16[1024,384]{1,0:T(8,128)(2,1)S(1)} %get-tuple-element.35.w_own, bf16[1024,384]{1,0:T(8,128)(2,1)S(1)} %collective-permute-done.w_got), custom_call_target="tpu_custom_call" | custom-call | flops 1207959552 | bytes 3019898 | tf_op jit(solution)/shard_map/pallas_call | solution.py:58
  54.9 1.9 %collective-permute-start.1 = (bf16[768,768]{1,0:T(8,128)(2,1)S(1)}, bf16[768,768]{1,0:T(8,128)(2,1)S(1)}, u32[]{:S(2)}, u32[]{:S(2)}) collective-permute-start(bf16[768,768]{1,0:T(8,128)(2,1)S(1)} %shard_map.112.part), channel_id=1, source_target_pairs={{0,1},{1,0},{2,3},{3,2},{4,5},{5,4},{6,7},{7,6},{8,9},{9,8},{10,11... | collective-permute-start | bytes 3538952 | tf_op jit(solution)/shard_map/ppermute | solution.py:392
  56.8 2.8 %collective-permute-done.1.got = bf16[768,768]{1,0:T(8,128)(2,1)S(1)} collective-permute-done((bf16[768,768]{1,0:T(8,128)(2,1)S(1)}, bf16[768,768]{1,0:T(8,128)(2,1)S(1)}, u32[]{:S(2)}, u32[]{:S(2)}) %collective-permute-start.1) | collective-permute-done | bytes 1179680 | tf_op jit(solution)/shard_map/ppermute | solution.py:392
  59.6 1.3 %shard_map.113 = (bf16[768,256]{1,0:T(8,128)(2,1)S(1)}, bf16[768,512]{1,0:T(8,128)(2,1)S(1)}, bf16[32,200,128]{2,1,0:T(8,128)(2,1)S(1)}) custom-call(s32[1]{0:T(128)} %bitcast.core, bf16[768,768]{1,0:T(8,128)(2,1)S(1)} %shard_map.112.part, bf16[768,768]{1,0:T(8,128)(2,1)S(1)} %collective-permute-done.1.got, bf16[1024,384]{1,0:T(8,128)(2,1)S(1)} %get-tuple-element.35.w_own, ...), custom_call_target="tpu_custom_call" | custom-call | flops 805306368 | bytes 2013265 | tf_op jit(solution)/shard_map/pallas_call | solution.py:58
  61.0 0.0 copy-start
  61.0 1.2 copy-done
  62.1 0.0 copy-start.3
  62.1 0.9 copy-done.3
  63.0 0.0 copy-start.5
  63.1 0.7 copy-done.5
  63.8 6.1 %all-to-all-start.1 = ((bf16[32,200,128]{2,1,0:T(8,128)(2,1)}), bf16[32,200,128]{2,1,0:T(8,128)(2,1)}, u32[]{:S(2)}, u32[]{:S(2)}) async-start(bf16[32,200,128]{2,1,0:T(8,128)(2,1)} %copy-done), calls=%async_computation.1 | async-start | bytes 3276800 | tf_op jit(solution)/shard_map/all_to_all | solution.py:397
  69.9 0.0 copy-start.4
  69.9 1.1 copy-done.4
  71.0 0.0 copy-start.6
  71.0 1.0 copy-done.6
  72.0 2.4 %shard_map.114 = (bf16[1024,384]{1,0:T(8,128)(2,1)S(1)}, bf16[1024,384]{1,0:T(8,128)(2,1)}) custom-call(s32[1]{0:T(128)} %bitcast.core, bf16[768,2048]{1,0:T(8,128)(2,1)S(1)} %bitcast.14, bf16[768,256]{1,0:T(8,128)(2,1)S(1)} %copy-done.6, bf16[768,512]{1,0:T(8,128)(2,1)S(1)} %copy-done.4), custom_call_target="tpu_custom_call" | custom-call | flops 1207959552 | bytes 3019898 | tf_op jit(solution)/shard_map/pallas_call | solution.py:58
  74.4 0.0 copy-start.1
  74.4 0.9 copy-done.1
  75.2 0.0 copy-start.2
  75.3 2.0 %collective-permute-start.2 = (bf16[1024,384]{1,0:T(8,128)(2,1)}, bf16[1024,384]{1,0:T(8,128)(2,1)S(1)}, u32[]{:S(2)}, u32[]{:S(2)}) collective-permute-start(bf16[1024,384]{1,0:T(8,128)(2,1)} %get-tuple-element.43), channel_id=1, source_target_pairs={{0,1},{1,0},{2,3},{3,2},{4,5},{5,4},{6,7},{7,6},{8,9},{9,8},{10,11... | collective-permute-start | bytes 2359304 | tf_op jit(solution)/shard_map/ppermute | solution.py:395
  77.3 17.0 %all-to-all-done.1.got = bf16[32,200,128]{2,1,0:T(8,128)(2,1)} async-done(((bf16[32,200,128]{2,1,0:T(8,128)(2,1)}), bf16[32,200,128]{2,1,0:T(8,128)(2,1)}, u32[]{:S(2)}, u32[]{:S(2)}) %all-to-all-start.1) | async-done | bytes 1638432 | tf_op jit(solution)/shard_map/all_to_all | solution.py:397
  94.3 2.9 %combine.1 = bf16[8,104,128]{2,1,0:T(8,128)(2,1)} custom-call(s32[2,192]{1,0:T(2,128)S(1)} %get-tuple-element.26.routes, f32[2,192]{1,0:T(2,128)S(1)} %get-tuple-element.27.weights, bf16[768,192]{1,0:T(8,128)(2,1)S(1)} %get-tuple-element.30.sel, bf16[32,200,128]{2,1,0:T(8,128)(2,1)} %all-to-all-done.1.got), custom_call_target="tpu_custom_call" | custom-call | tf_op jit(solution)/shard_map/combine/pallas_call | solution.py:329
  97.2 13.4 %all-to-all-start.2 = ((bf16[8,104,128]{2,1,0:T(8,128)(2,1)}), bf16[8,104,128]{2,1,0:T(8,128)(2,1)S(1)}, u32[]{:S(2)}, u32[]{:S(2)}) async-start(bf16[8,104,128]{2,1,0:T(8,128)(2,1)} %combine.1), calls=%async_computation.2 | async-start | bytes 425984 | tf_op jit(solution)/shard_map/all_to_all | solution.py:399
  110.6 0.0 collective-permute-done.2.got
  110.6 0.0 copy-done.2
  110.6 1.5 %shard_map.115 = (bf16[2048,128]{1,0:T(8,128)(2,1)}, bf16[2048,128]{1,0:T(8,128)(2,1)}, bf16[128,2048]{1,0:T(8,128)(2,1)}) custom-call(s32[1]{0:T(128)} %bitcast.core, bf16[1024,384]{1,0:T(8,128)(2,1)S(1)} %copy-done.2, bf16[1024,384]{1,0:T(8,128)(2,1)S(1)} %collective-permute-done.2.got), custom_call_target="tpu_custom_call" | custom-call | flops 268435456 | bytes 671088 | tf_op jit(solution)/shard_map/pallas_call | solution.py:58
  112.1 15.6 %all-to-all-done.2.got = bf16[8,104,128]{2,1,0:T(8,128)(2,1)S(1)} async-done(((bf16[8,104,128]{2,1,0:T(8,128)(2,1)}), bf16[8,104,128]{2,1,0:T(8,128)(2,1)S(1)}, u32[]{:S(2)}, u32[]{:S(2)}) %all-to-all-start.2) | async-done | bytes 213024 | tf_op jit(solution)/shard_map/all_to_all | solution.py:399
  127.7 0.8 finish.1
Async XLA Ops:
  2.6 4.2 %collective-permute-start = (bf16[1024,384]{1,0:T(8,128)(2,1)S(1)}, bf16[1024,384]{1,0:T(8,128)(2,1)S(1)}, u32[]{:S(2)}, u32[]{:S(2)}) collective-permute-start(bf16[1024,384]{1,0:T(8,128)(2,1)S(1)} %get-tuple-element.33), channel_id=1, source_target_pairs={{0,1},{1,0},{2,3},{3,2},{4,5},{5,4},{6,7},{7,6},{8,9},{9,8},{10,11... | collective-permute-start | bytes 2359304 | tf_op jit(solution)/shard_map/ppermute | solution.py:387
  54.9 4.7 %collective-permute-start.1 = (bf16[768,768]{1,0:T(8,128)(2,1)S(1)}, bf16[768,768]{1,0:T(8,128)(2,1)S(1)}, u32[]{:S(2)}, u32[]{:S(2)}) collective-permute-start(bf16[768,768]{1,0:T(8,128)(2,1)S(1)} %shard_map.112.part), channel_id=1, source_target_pairs={{0,1},{1,0},{2,3},{3,2},{4,5},{5,4},{6,7},{7,6},{8,9},{9,8},{10,11... | collective-permute-start | bytes 3538952 | tf_op jit(solution)/shard_map/ppermute | solution.py:392
  61.0 1.2 copy-start
  62.1 0.9 copy-start.3
  63.0 0.7 copy-start.5
  63.8 30.5 %all-to-all-start.1 = ((bf16[32,200,128]{2,1,0:T(8,128)(2,1)}), bf16[32,200,128]{2,1,0:T(8,128)(2,1)}, u32[]{:S(2)}, u32[]{:S(2)}) async-start(bf16[32,200,128]{2,1,0:T(8,128)(2,1)} %copy-done), calls=%async_computation.1 | async-start | bytes 3276800 | tf_op jit(solution)/shard_map/all_to_all | solution.py:397
  69.9 1.1 copy-start.4
  71.0 1.0 copy-start.6
  74.4 0.9 copy-start.1
  75.2 35.4 %copy-start.2 = (bf16[1024,384]{1,0:T(8,128)(2,1)S(1)}, bf16[1024,384]{1,0:T(8,128)(2,1)}, u32[]{:S(2)}) copy-start(bf16[1024,384]{1,0:T(8,128)(2,1)} %copy-done.1) | copy-start | bytes 2359300
  75.3 35.4 %collective-permute-start.2 = (bf16[1024,384]{1,0:T(8,128)(2,1)}, bf16[1024,384]{1,0:T(8,128)(2,1)S(1)}, u32[]{:S(2)}, u32[]{:S(2)}) collective-permute-start(bf16[1024,384]{1,0:T(8,128)(2,1)} %get-tuple-element.43), channel_id=1, source_target_pairs={{0,1},{1,0},{2,3},{3,2},{4,5},{5,4},{6,7},{7,6},{8,9},{9,8},{10,11... | collective-permute-start | bytes 2359304 | tf_op jit(solution)/shard_map/ppermute | solution.py:395
  97.2 30.6 %all-to-all-start.2 = ((bf16[8,104,128]{2,1,0:T(8,128)(2,1)}), bf16[8,104,128]{2,1,0:T(8,128)(2,1)S(1)}, u32[]{:S(2)}, u32[]{:S(2)}) async-start(bf16[8,104,128]{2,1,0:T(8,128)(2,1)} %combine.1), calls=%async_computation.2 | async-start | bytes 425984 | tf_op jit(solution)/shard_map/all_to_all | solution.py:399
where the time goes:
time: 129 us
  blocking collectives  46.7 us (36%)
  waiting for transfers between devices  36 us (28%)
  starting transfers between devices  25.4 us (20%)
  Pallas kernels  13.9 us (11%)
  local copies, waits for them, and re-layouts  5.81 us (5%)
    all_to_all x1, blocking collectives, shards(): lax.all_to_all(packed.reshape(experts, cap, d), 'ep', 0, 0, tiled=True)  46.7 us
    all_to_all x1, waiting for transfers between devices, shards(): back = lax.all_to_all(message, ('ep', 'zl'), 0, 0, tiled=True)  17 us
    all_to_all x1, waiting for transfers between devices, shards(): last = lax.all_to_all(partial, 'zh', 0, 0, tiled=True)  15.6 us
    all_to_all x1, starting transfers between devices, shards(): last = lax.all_to_all(partial, 'zh', 0, 0, tiled=True)  13.4 us
    pallas_call x6, Pallas kernels, call(): pl.pallas_call(kernel, in_specs=[pl.BlockSpec(memory_space=pltpu.SMEM)] +...  10.1 us
    all_to_all x1, starting transfers between devices, shards(): back = lax.all_to_all(message, ('ep', 'zl'), 0, 0, tiled=True)  6.06 us
    unnamed x14, local copies, waits for them, and re-layouts  5.81 us
    pallas_call x1, Pallas kernels, combine(): pl.pallas_call(functools.partial(combine_kernel, experts=experts, cap=cap...  2.92 us
  transfers between devices with their start and end apart: 5, of which 4 were waited for; matrix products, arithmetic and copies ran while one was open for 0% of the time, Pallas kernels for 7%

commit v1 on v0

--- a/solution.py
+++ b/solution.py
@@ -209,12 +209,13 @@
             act = a * s
             hidden = (act * b).astype(BF)
             hid[at, pl.ds(k * LANES, LANES)] = hidden
-            dd[at, pl.ds(2 * k * LANES, LANES)] = (back * b * s * (1.0 + a * (1.0 - s))).astype(BF)
-            dd[at, pl.ds((2 * k + 1) * LANES, LANES)] = (back * act).astype(BF)
+            da = (back * b * s * (1.0 + a * (1.0 - s))).astype(BF)
+            both = jnp.concatenate([da, (back * act).astype(BF)], axis=1)
+            dd[at, pl.ds(2 * k * LANES, 2 * LANES)] = both
+            term = dot(both, (w_own, w_got)[k][:, pl.ds(0, 2 * LANES)], 1, 1)
+            rows = term if k == 0 else rows + term
             one = jnp.sum((hidden.astype(F32) * back).T, axis=0, keepdims=True)
             route = one if route is None else route + one
-        rows = dot(dd[at, pl.ds(0, 2 * LANES)], w_own[:, pl.ds(0, 2 * LANES)], 1, 1)
-        rows = rows + dot(dd[at, pl.ds(2 * LANES, 2 * LANES)], w_got[:, pl.ds(0, 2 * LANES)], 1, 1)
         rows = rows.astype(BF)
         for j in range(group // cap):
             b = i * (group // cap) + j
@@ -222,10 +223,10 @@
             for zl in range(nzl):
                 for q in range(per):
                     k = zl * per + q
-                    out[b * nzl + zl, pl.ds(q * cap, cap), :] = rows[
+                    out[zl * (slots // cap) + b, pl.ds(q * cap, cap), :] = rows[
                         j * cap : (j + 1) * cap, k * LANES : (k + 1) * LANES
                     ]
-                out[b * nzl + zl, pl.ds(per * cap, 8), :] = ends
+                out[zl * (slots // cap) + b, pl.ds(per * cap, 8), :] = ends
 
 
 def backward(core, part, got, w_own, w_got, nzl, cap):
@@ -287,7 +288,7 @@
         for e in range(experts):
             for q in range(per):
                 part[zl, pl.ds(e * cap, cap), pl.ds(q * LANES, LANES)] = got[
-                    e * nzl + zl, pl.ds(q * cap, cap), :
+                    zl * experts + e, pl.ds(q * cap, cap), :
                 ]
         one = dot(s, part[zl], 0, 0)
         total = one if total is None else total + one
@@ -301,7 +302,7 @@
     for e in range(experts):
         line = jnp.zeros((1, LANES), F32)
         for zl in range(nzl):
-            tail = got[e * nzl + zl, pl.ds(per * cap, 8), :].astype(F32)
+            tail = got[zl * experts + e, pl.ds(per * cap, 8), :].astype(F32)
             line = line + tail[0:1] + tail[1:2]
         lines.append(line)
     r_hi, r_lo = split(stacked(lines, max(experts, 8)))
@@ -394,7 +395,7 @@
     keep, send = grads(core, own, hid, dd)
     moved = lax.ppermute(send, "core", swap)
     gg, gu, gd = place(core, keep, moved, nzh, nzl)
-    back = lax.all_to_all(message, ("ep", "zl"), 0, 0, tiled=True)
+    back = lax.all_to_all(message, ("zl", "ep"), 0, 0, tiled=True)
     partial = combine(routes_v, weight_v, sel, back, experts, cap, nzh, nzl)
     last = lax.all_to_all(partial, "zh", 0, 0, tiled=True)
     grad_t, route_t = finish(last, rows)

time: 129 us -> 129 us (level)
  the two profiles are of different devices: /device:TPU:32 before, /device:TPU:2 now
where the time goes in v1:
time: 129 us; the launch traced here: 128 us
  blocking collectives  47.5 us (37%)
  waiting for transfers between devices  35.5 us (28%)
  starting transfers between devices  25.1 us (19%)
  Pallas kernels  13.9 us (11%)
  local copies, waits for them, and re-layouts  5.81 us (5%)
    all_to_all x1, blocking collectives, shards(): lax.all_to_all(packed.reshape(experts, cap, d), 'ep', 0, 0, tiled=True)  47.5 us
    all_to_all x1, waiting for transfers between devices, shards(): last = lax.all_to_all(partial, 'zh', 0, 0, tiled=True)  16.9 us
    all_to_all x1, waiting for transfers between devices, shards(): back = lax.all_to_all(message, ('zl', 'ep'), 0, 0, tiled=True)  15.2 us
    all_to_all x1, starting transfers between devices, shards(): last = lax.all_to_all(partial, 'zh', 0, 0, tiled=True)  13.4 us
    pallas_call x6, Pallas kernels, call(): pl.pallas_call(kernel, in_specs=[pl.BlockSpec(memory_space=pltpu.SMEM)] +...  10.1 us
    unnamed x14, local copies, waits for them, and re-layouts  5.81 us
    all_to_all x1, starting transfers between devices, shards(): back = lax.all_to_all(message, ('zl', 'ep'), 0, 0, tiled=True)  5.76 us
    pallas_call x1, Pallas kernels, combine(): pl.pallas_call(functools.partial(combine_kernel, experts=experts, cap=cap...  2.92 us
  transfers between devices with their start and end apart: 5, of which 4 were waited for; matrix products, arithmetic and copies ran while one was open for 0% of the time, Pallas kernels for 7%

profile of v1, /device:TPU:2, one launch (start us, length us, event | category | flops | bytes accessed | tf_op | source)
XLA Modules:
  0.0 128.5 jit_solution(15279653776670667306)
XLA Ops:
  0.6 1.9 %shard_map.110 = (s32[2,192]{1,0:T(2,128)S(1)}, f32[2,192]{1,0:T(2,128)S(1)}, bf16[192,2048]{1,0:T(8,128)(2,1)S(1)}, bf16[192,2048]{1,0:T(8,128)(2,1)S(1)}, bf16...) custom-call(s32[1]{0:T(128)} %bitcast.core, s32[2,192]{1,0:T(2,128)} %bitcast.19, f32[2,192]{1,0:T(2,128)} %bitcast.20, ...), custom_call_target="tpu_custom_call" | custom-call | flops 268435456 | bytes 671088 | tf_op jit(solution)/shard_map/pallas_call | solution.py:58
  2.6 1.9 %collective-permute-start = (bf16[1024,384]{1,0:T(8,128)(2,1)S(1)}, bf16[1024,384]{1,0:T(8,128)(2,1)S(1)}, u32[]{:S(2)}, u32[]{:S(2)}) collective-permute-start(bf16[1024,384]{1,0:T(8,128)(2,1)S(1)} %get-tuple-element.33), channel_id=1, source_target_pairs={{0,1},{1,0},{2,3},{3,2},{4,5},{5,4},{6,7},{7,6},{8,9},{9,8},{10,11... | collective-permute-start | bytes 2359304 | tf_op jit(solution)/shard_map/ppermute | solution.py:388
  4.5 1.6 %shard_map.111 = (bf16[768,2048]{1,0:T(8,128)(2,1)S(1)}, bf16[768,192]{1,0:T(8,128)(2,1)S(1)}) custom-call(s32[1]{0:T(128)} %bitcast.core, s32[2,192]{1,0:T(2,128)S(1)} %get-tuple-element.26.routes, f32[2,192]{1,0:T(2,128)S(1)} %get-tuple-element.27.weights, bf16[192,2048]{1,0:T(8,128)(2,1)S(1)} %get-tuple-element.28.x, ...), custom_call_target="tpu_custom_call" | custom-call | flops 603979776 | bytes 1509949 | tf_op jit(solution)/shard_map/pallas_call | solution.py:58
  6.1 0.6 collective-permute-done.w_got
  6.8 47.5 %all_to_all.15 = bf16[16,48,2048]{2,1,0:T(8,128)(2,1)S(1)} all-to-all(bf16[16,48,2048]{2,1,0:T(8,128)(2,1)S(1)} %bitcast.15), channel_id=1, replica_groups=mesh['ep'=16,'zh'=8,'zl'=2,'core'=2] {'ep'}, dimensions={0} | all-to-all | bytes 6291456 | tf_op jit(solution)/shard_map/all_to_all | solution.py:391
  54.2 1.4 %shard_map.112.part = bf16[768,768]{1,0:T(8,128)(2,1)S(1)} custom-call(s32[1]{0:T(128)} %bitcast.core, bf16[768,2048]{1,0:T(8,128)(2,1)S(1)} %bitcast.13, bf16[1024,384]{1,0:T(8,128)(2,1)S(1)} %get-tuple-element.35.w_own, bf16[1024,384]{1,0:T(8,128)(2,1)S(1)} %collective-permute-done.w_got), custom_call_target="tpu_custom_call" | custom-call | flops 1207959552 | bytes 3019898 | tf_op jit(solution)/shard_map/pallas_call | solution.py:58
  55.6 1.9 %collective-permute-start.1 = (bf16[768,768]{1,0:T(8,128)(2,1)S(1)}, bf16[768,768]{1,0:T(8,128)(2,1)S(1)}, u32[]{:S(2)}, u32[]{:S(2)}) collective-permute-start(bf16[768,768]{1,0:T(8,128)(2,1)S(1)} %shard_map.112.part), channel_id=1, source_target_pairs={{0,1},{1,0},{2,3},{3,2},{4,5},{5,4},{6,7},{7,6},{8,9},{9,8},{10,11... | collective-permute-start | bytes 3538952 | tf_op jit(solution)/shard_map/ppermute | solution.py:393
  57.6 2.8 %collective-permute-done.1.got = bf16[768,768]{1,0:T(8,128)(2,1)S(1)} collective-permute-done((bf16[768,768]{1,0:T(8,128)(2,1)S(1)}, bf16[768,768]{1,0:T(8,128)(2,1)S(1)}, u32[]{:S(2)}, u32[]{:S(2)}) %collective-permute-start.1) | collective-permute-done | bytes 1179680 | tf_op jit(solution)/shard_map/ppermute | solution.py:393
  60.4 1.3 %shard_map.113 = (bf16[768,256]{1,0:T(8,128)(2,1)S(1)}, bf16[768,512]{1,0:T(8,128)(2,1)S(1)}, bf16[32,200,128]{2,1,0:T(8,128)(2,1)S(1)}) custom-call(s32[1]{0:T(128)} %bitcast.core, bf16[768,768]{1,0:T(8,128)(2,1)S(1)} %shard_map.112.part, bf16[768,768]{1,0:T(8,128)(2,1)S(1)} %collective-permute-done.1.got, bf16[1024,384]{1,0:T(8,128)(2,1)S(1)} %get-tuple-element.35.w_own, ...), custom_call_target="tpu_custom_call" | custom-call | flops 805306368 | bytes 2013265 | tf_op jit(solution)/shard_map/pallas_call | solution.py:58
  61.7 0.0 copy-start
  61.7 1.2 copy-done
  62.9 0.0 copy-start.3
  62.9 0.9 copy-done.3
  63.8 0.0 copy-start.5
  63.8 0.7 copy-done.5
  64.5 5.8 %all-to-all-start.1 = ((bf16[32,200,128]{2,1,0:T(8,128)(2,1)}), bf16[32,200,128]{2,1,0:T(8,128)(2,1)}, u32[]{:S(2)}, u32[]{:S(2)}) async-start(bf16[32,200,128]{2,1,0:T(8,128)(2,1)} %copy-done), calls=%async_computation.1 | async-start | bytes 3276800 | tf_op jit(solution)/shard_map/all_to_all | solution.py:398
  70.3 0.0 copy-start.4
  70.3 1.1 copy-done.4
  71.4 0.0 copy-start.6
  71.4 1.0 copy-done.6
  72.4 2.4 %shard_map.114 = (bf16[1024,384]{1,0:T(8,128)(2,1)S(1)}, bf16[1024,384]{1,0:T(8,128)(2,1)}) custom-call(s32[1]{0:T(128)} %bitcast.core, bf16[768,2048]{1,0:T(8,128)(2,1)S(1)} %bitcast.14, bf16[768,256]{1,0:T(8,128)(2,1)S(1)} %copy-done.6, bf16[768,512]{1,0:T(8,128)(2,1)S(1)} %copy-done.4), custom_call_target="tpu_custom_call" | custom-call | flops 1207959552 | bytes 3019898 | tf_op jit(solution)/shard_map/pallas_call | solution.py:58
  74.8 0.0 copy-start.1
  74.8 0.9 copy-done.1
  75.7 0.0 copy-start.2
  75.7 2.0 %collective-permute-start.2 = (bf16[1024,384]{1,0:T(8,128)(2,1)}, bf16[1024,384]{1,0:T(8,128)(2,1)S(1)}, u32[]{:S(2)}, u32[]{:S(2)}) collective-permute-start(bf16[1024,384]{1,0:T(8,128)(2,1)} %get-tuple-element.43), channel_id=1, source_target_pairs={{0,1},{1,0},{2,3},{3,2},{4,5},{5,4},{6,7},{7,6},{8,9},{9,8},{10,11... | collective-permute-start | bytes 2359304 | tf_op jit(solution)/shard_map/ppermute | solution.py:396
  77.7 15.2 %all-to-all-done.1.got = bf16[32,200,128]{2,1,0:T(8,128)(2,1)} async-done(((bf16[32,200,128]{2,1,0:T(8,128)(2,1)}), bf16[32,200,128]{2,1,0:T(8,128)(2,1)}, u32[]{:S(2)}, u32[]{:S(2)}) %all-to-all-start.1) | async-done | bytes 1638432 | tf_op jit(solution)/shard_map/all_to_all | solution.py:398
  92.9 2.9 %combine.1 = bf16[8,104,128]{2,1,0:T(8,128)(2,1)} custom-call(s32[2,192]{1,0:T(2,128)S(1)} %get-tuple-element.26.routes, f32[2,192]{1,0:T(2,128)S(1)} %get-tuple-element.27.weights, bf16[768,192]{1,0:T(8,128)(2,1)S(1)} %get-tuple-element.30.sel, bf16[32,200,128]{2,1,0:T(8,128)(2,1)} %all-to-all-done.1.got), custom_call_target="tpu_custom_call" | custom-call | tf_op jit(solution)/shard_map/combine/pallas_call | solution.py:330
  95.9 13.4 %all-to-all-start.2 = ((bf16[8,104,128]{2,1,0:T(8,128)(2,1)}), bf16[8,104,128]{2,1,0:T(8,128)(2,1)S(1)}, u32[]{:S(2)}, u32[]{:S(2)}) async-start(bf16[8,104,128]{2,1,0:T(8,128)(2,1)} %combine.1), calls=%async_computation.2 | async-start | bytes 425984 | tf_op jit(solution)/shard_map/all_to_all | solution.py:400
  109.3 0.0 collective-permute-done.2.got
  109.3 0.0 copy-done.2
  109.3 1.5 %shard_map.115 = (bf16[2048,128]{1,0:T(8,128)(2,1)}, bf16[2048,128]{1,0:T(8,128)(2,1)}, bf16[128,2048]{1,0:T(8,128)(2,1)}) custom-call(s32[1]{0:T(128)} %bitcast.core, bf16[1024,384]{1,0:T(8,128)(2,1)S(1)} %copy-done.2, bf16[1024,384]{1,0:T(8,128)(2,1)S(1)} %collective-permute-done.2.got), custom_call_target="tpu_custom_call" | custom-call | flops 268435456 | bytes 671088 | tf_op jit(solution)/shard_map/pallas_call | solution.py:58
  110.8 16.9 %all-to-all-done.2.got = bf16[8,104,128]{2,1,0:T(8,128)(2,1)S(1)} async-done(((bf16[8,104,128]{2,1,0:T(8,128)(2,1)}), bf16[8,104,128]{2,1,0:T(8,128)(2,1)S(1)}, u32[]{:S(2)}, u32[]{:S(2)}) %all-to-all-start.2) | async-done | bytes 213024 | tf_op jit(solution)/shard_map/all_to_all | solution.py:400
  127.7 0.8 finish.1
Async XLA Ops:
  2.6 4.2 %collective-permute-start = (bf16[1024,384]{1,0:T(8,128)(2,1)S(1)}, bf16[1024,384]{1,0:T(8,128)(2,1)S(1)}, u32[]{:S(2)}, u32[]{:S(2)}) collective-permute-start(bf16[1024,384]{1,0:T(8,128)(2,1)S(1)} %get-tuple-element.33), channel_id=1, source_target_pairs={{0,1},{1,0},{2,3},{3,2},{4,5},{5,4},{6,7},{7,6},{8,9},{9,8},{10,11... | collective-permute-start | bytes 2359304 | tf_op jit(solution)/shard_map/ppermute | solution.py:388
  55.6 4.7 %collective-permute-start.1 = (bf16[768,768]{1,0:T(8,128)(2,1)S(1)}, bf16[768,768]{1,0:T(8,128)(2,1)S(1)}, u32[]{:S(2)}, u32[]{:S(2)}) collective-permute-start(bf16[768,768]{1,0:T(8,128)(2,1)S(1)} %shard_map.112.part), channel_id=1, source_target_pairs={{0,1},{1,0},{2,3},{3,2},{4,5},{5,4},{6,7},{7,6},{8,9},{9,8},{10,11... | collective-permute-start | bytes 3538952 | tf_op jit(solution)/shard_map/ppermute | solution.py:393
  61.7 1.2 copy-start
  62.9 0.9 copy-start.3
  63.8 0.7 copy-start.5
  64.5 28.4 %all-to-all-start.1 = ((bf16[32,200,128]{2,1,0:T(8,128)(2,1)}), bf16[32,200,128]{2,1,0:T(8,128)(2,1)}, u32[]{:S(2)}, u32[]{:S(2)}) async-start(bf16[32,200,128]{2,1,0:T(8,128)(2,1)} %copy-done), calls=%async_computation.1 | async-start | bytes 3276800 | tf_op jit(solution)/shard_map/all_to_all | solution.py:398
  70.3 1.1 copy-start.4
  71.4 1.0 copy-start.6
  74.8 0.9 copy-start.1
  75.7 33.6 %copy-start.2 = (bf16[1024,384]{1,0:T(8,128)(2,1)S(1)}, bf16[1024,384]{1,0:T(8,128)(2,1)}, u32[]{:S(2)}) copy-start(bf16[1024,384]{1,0:T(8,128)(2,1)} %copy-done.1) | copy-start | bytes 2359300
  75.7 33.6 %collective-permute-start.2 = (bf16[1024,384]{1,0:T(8,128)(2,1)}, bf16[1024,384]{1,0:T(8,128)(2,1)S(1)}, u32[]{:S(2)}, u32[]{:S(2)}) collective-permute-start(bf16[1024,384]{1,0:T(8,128)(2,1)} %get-tuple-element.43), channel_id=1, source_target_pairs={{0,1},{1,0},{2,3},{3,2},{4,5},{5,4},{6,7},{7,6},{8,9},{9,8},{10,11... | collective-permute-start | bytes 2359304 | tf_op jit(solution)/shard_map/ppermute | solution.py:396
  95.9 31.8 %all-to-all-start.2 = ((bf16[8,104,128]{2,1,0:T(8,128)(2,1)}), bf16[8,104,128]{2,1,0:T(8,128)(2,1)S(1)}, u32[]{:S(2)}, u32[]{:S(2)}) async-start(bf16[8,104,128]{2,1,0:T(8,128)(2,1)} %combine.1), calls=%async_computation.2 | async-start | bytes 425984 | tf_op jit(solution)/shard_map/all_to_all | solution.py:400
